TPU v7x, 32 devices: a whole 2x2x4 slice. The times are simulated.
32 devices in a mesh: rep: 2 (over x), fs: 8 (over z, y), tp: 2 (over core).
Axes of the slice: x: 2, y: 2, z: 4, core: 2. Of those that a mesh axis runs over, the one named last changes fastest.
Arguments:
- activations: bfloat16 [3072, 2048], P(('rep', 'fs'), 'tp'), may hold values from -6 to 6
- mix_gain: float32 [2048], replicated, may hold values from 0.1 to 1.9
- mlp_gain: float32 [2048], replicated, may hold values from 0.1 to 1.9
- query_weight: float32 [2048, 512], P('fs', 'tp'), may hold values from -0.125 to 0.125
- query_scale: float32 [512], P('tp'), may hold values from 0.3 to 3
- key_weight: float32 [2048, 512], P('fs', 'tp'), may hold values from -0.125 to 0.125
- key_scale: float32 [512], P('tp'), may hold values from 0.3 to 3
- value_weight: float32 [2048, 1024], P('fs', 'tp'), may hold values from -0.125 to 0.125
- value_scale: float32 [1024], P('tp'), may hold values from 0.3 to 3
- gate_weight: float32 [2048, 1024], P('fs', 'tp'), may hold values from -0.125 to 0.125
- gate_scale: float32 [1024], P('tp'), may hold values from 0.3 to 3
- out_weight: float32 [1024, 2048], P('tp', 'fs'), may hold values from -0.1875 to 0.1875
- out_scale: float32 [2048], P('fs'), may hold values from 0.3 to 3
- up_weight: float32 [2048, 8192], P('fs', 'tp'), may hold values from -0.125 to 0.125
- up_scale: float32 [8192], P('tp'), may hold values from 0.3 to 3
- down_weight: float32 [8192, 2048], P('tp', 'fs'), may hold values from -0.0625 to 0.0625
- down_scale: float32 [2048], P('fs'), may hold values from 0.3 to 3
- log_decay: float32 [8], P('tp'), may hold values from -0.1 to 0, as said below
Outputs:
- result: bfloat16 [3072, 2048], P(('rep', 'fs'), 'tp')
Inputs may be any that keep to these rules, and one draw needn't show every extreme that they name: `log_decay`: negative for every head.
All inputs are finite; a program needn't handle non-finite values.
Results may differ from a plain program's by a relative error of at most 0.023.
Values may be sent and summed in bfloat16 or wider, within the bound.
A program may use at most 128 MiB of HBM per device.

v0:
```python
import jax
import jax.numpy as jnp
from jax import lax
from jax.sharding import PartitionSpec as P

BLOCK = 64
LENGTH = 192
epsilon = 1e-06
rope_base = 10000.0


def rotate(head_rows, positions):
    half = head_rows.shape[-1] // 2
    inverse = 1.0 / rope_base ** jnp.linspace(0.0, 1.0, half, dtype=jnp.float32)
    angles = positions[:, None] * inverse[None, :]
    cosine = jnp.cos(angles)[:, None, :]
    sine = jnp.sin(angles)[:, None, :]
    first = head_rows[..., :half]
    second = head_rows[..., half:]
    return jnp.concatenate(
        [first * cosine - second * sine, first * sine + second * cosine], axis=-1
    )


def retain(query_heads, key_heads, value_heads, log_decay):
    batch, length, heads, width = query_heads.shape
    block_count = length // BLOCK
    highest = lax.Precision.HIGHEST

    def to_blocks(tensor):
        return tensor.reshape(batch, block_count, BLOCK, heads, tensor.shape[-1]).transpose(
            0, 3, 1, 2, 4
        )

    query_blocks = to_blocks(query_heads)
    key_blocks = to_blocks(key_heads)
    value_blocks = to_blocks(value_heads)
    places = jnp.arange(BLOCK, dtype=jnp.float32)
    offsets = places[:, None] - places[None, :]
    inner = jnp.where(
        offsets >= 0, jnp.exp(log_decay[:, None, None] * jnp.maximum(offsets, 0.0)), 0.0
    )
    scores = (
        jnp.einsum("bhntd,bhnsd->bhnts", query_blocks, key_blocks, precision=highest)
        * inner[None, :, None]
    )
    output = jnp.einsum("bhnts,bhnse->bhnte", scores, value_blocks, precision=highest)
    keys_decayed = (
        key_blocks
        * jnp.exp(log_decay[:, None] * (BLOCK - 1.0 - places)[None, :])[None, :, None, :, None]
    )
    increments = jnp.einsum("bhnsd,bhnse->nbhde", keys_decayed, value_blocks, precision=highest)
    carry_decay = jnp.exp(log_decay * BLOCK)[None, :, None, None]

    def advance(state, increment):
        return (carry_decay * state + increment, state)

    initial = jnp.zeros((batch, heads, width, value_heads.shape[-1]), jnp.float32)
    _, states = lax.scan(advance, initial, increments)
    query_decayed = (
        query_blocks * jnp.exp(log_decay[:, None] * (places + 1.0)[None, :])[None, :, None, :, None]
    )
    output = output + jnp.einsum("bhntd,nbhde->bhnte", query_decayed, states, precision=highest)
    return output.transpose(0, 2, 3, 1, 4).reshape(batch, length, heads, value_heads.shape[-1])


def gather_norm(rows, gain):
    whole = lax.all_gather(rows, "tp", axis=1, tiled=True)
    wide = whole.astype(jnp.float32)
    mean_square = jnp.mean(wide * wide, axis=1, keepdims=True)
    return (wide * lax.rsqrt(mean_square + epsilon) * gain).astype(jnp.bfloat16)


def column_terms(weight, scale, hidden):
    partial_value = lax.dot_general(
        weight, hidden, (((0,), (1,)), ((), ())), preferred_element_type=jnp.float32
    )
    return partial_value * scale[:, None]


def on_device(
    activations,
    mix_gain,
    mlp_gain,
    query_weight,
    query_scale,
    key_weight,
    key_scale,
    value_weight,
    value_scale,
    gate_weight,
    gate_scale,
    out_weight,
    out_scale,
    up_weight,
    up_scale,
    down_weight,
    down_scale,
    log_decay,
):
    query_full, key_full, value_full, gate_full, out_full = (
        lax.all_gather(query_weight.astype(jnp.bfloat16), "fs", axis=0, tiled=True),
        lax.all_gather(key_weight.astype(jnp.bfloat16), "fs", axis=0, tiled=True),
        lax.all_gather(value_weight.astype(jnp.bfloat16), "fs", axis=0, tiled=True),
        lax.all_gather(gate_weight.astype(jnp.bfloat16), "fs", axis=0, tiled=True),
        lax.all_gather(out_weight.astype(jnp.bfloat16), "fs", axis=1, tiled=True),
    )
    out_columns, down_columns = (
        lax.all_gather(out_scale, "fs", axis=0, tiled=True),
        lax.all_gather(down_scale, "fs", axis=0, tiled=True),
    )
    normed = gather_norm(activations, mix_gain)
    total_rows = normed.shape[0]
    sequences = total_rows // LENGTH
    heads = log_decay.shape[0]
    query = jnp.dot(normed, query_full, preferred_element_type=jnp.float32) * query_scale
    key_rows = jnp.dot(normed, key_full, preferred_element_type=jnp.float32) * key_scale
    value = jnp.dot(normed, value_full, preferred_element_type=jnp.float32) * value_scale
    gate = jnp.dot(normed, gate_full, preferred_element_type=jnp.float32) * gate_scale
    positions = jnp.arange(LENGTH, dtype=jnp.float32)
    query_heads = rotate(query.reshape(sequences, LENGTH, heads, -1), positions)
    key_heads = rotate(key_rows.reshape(sequences, LENGTH, heads, -1), positions)
    value_heads = value.reshape(sequences, LENGTH, heads, -1)
    retained = retain(query_heads, key_heads, value_heads, log_decay)
    retained = retained * lax.rsqrt(jnp.mean(retained * retained, axis=-1, keepdims=True) + epsilon)
    attended = (retained.reshape(total_rows, -1) * jax.nn.silu(gate)).astype(jnp.bfloat16)
    mixed = lax.psum_scatter(
        column_terms(out_full, out_columns, attended).astype(jnp.bfloat16),
        "tp",
        scatter_dimension=0,
        tiled=True,
    ).astype(jnp.float32)
    first = (activations.astype(jnp.float32) + mixed.T).astype(jnp.bfloat16)
    normed_two = gather_norm(first, mlp_gain)
    up_full, down_full = (
        lax.all_gather(up_weight.astype(jnp.bfloat16), "fs", axis=0, tiled=True),
        lax.all_gather(down_weight.astype(jnp.bfloat16), "fs", axis=1, tiled=True),
    )
    raised = jnp.dot(normed_two, up_full, preferred_element_type=jnp.float32) * up_scale
    hidden = jnp.square(jax.nn.relu(raised)).astype(jnp.bfloat16)
    channel = lax.psum_scatter(
        column_terms(down_full, down_columns, hidden).astype(jnp.bfloat16),
        "tp",
        scatter_dimension=0,
        tiled=True,
    ).astype(jnp.float32)
    return (first.astype(jnp.float32) + channel.T).astype(jnp.bfloat16)


def solution(mesh):
    placed = (
        P(("rep", "fs"), "tp"),
        P(),
        P(),
        P("fs", "tp"),
        P("tp"),
        P("fs", "tp"),
        P("tp"),
        P("fs", "tp"),
        P("tp"),
        P("fs", "tp"),
        P("tp"),
        P("tp", "fs"),
        P("fs"),
        P("fs", "tp"),
        P("tp"),
        P("tp", "fs"),
        P("fs"),
        P("tp"),
    )
    return jax.shard_map(
        on_device, mesh=mesh, in_specs=placed, out_specs=P(("rep", "fs"), "tp"), check_vma=False
    )
```

profile of v0, /device:TPU:0, one launch (start us, length us, event | category | flops | bytes accessed | tf_op | source)
XLA Modules:
  0.0 743.4 jit_solution(15880534284613785428)
XLA Ops:
  6.5 1.7 convert_element_type.68
  10.0 1.8 convert_element_type.70
  13.8 2.5 all_gather.33
  17.0 22.2 %all-gather = f32[8,1,256]{2,1,0:T(1,128)S(1)} all-gather(f32[1,1,256]{2,1,0:T(1,128)S(1)} %bitcast.109), channel_id=1, replica_groups=mesh['rep'=2,'fs'=8,'tp'=2] {'fs'}, dimensions={0}, use_global_device_ids=true | all-gather | bytes 9216 | tf_op jit(solution)/shard_map/all_gather | solution.py:109
  39.2 13.4 %all-gather.10.cloned.1.call-done = bf16[2048,256]{1,0:T(8,128)(2,1)} async-done(((bf16[256,256]{1,0:T(8,128)(2,1)}), bf16[2048,256]{1,0:T(8,128)(2,1)}) %all-gather.10.cloned.1.call-update) | async-done | bytes 1048592 | tf_op jit(solution)/shard_map/all_gather | solution.py:102
  52.6 1.6 convolution_multiply_fusion.7
  54.4 39.3 %all-gather.12.cloned.1.call-done = bf16[2048,256]{1,0:T(8,128)(2,1)} async-done(((bf16[256,256]{1,0:T(8,128)(2,1)}), bf16[2048,256]{1,0:T(8,128)(2,1)}) %all-gather.12.cloned.1.call-update) | async-done | bytes 1048592 | tf_op jit(solution)/shard_map/all_gather | solution.py:103
  93.8 1.6 convolution_multiply_fusion.6
  96.8 46.9 %all-gather.14.cloned.1.call-done = bf16[2048,512]{1,0:T(8,128)(2,1)} async-done(((bf16[256,512]{1,0:T(8,128)(2,1)}), bf16[2048,512]{1,0:T(8,128)(2,1)}) %all-gather.14.cloned.1.call-update) | async-done | bytes 2097168 | tf_op jit(solution)/shard_map/all_gather | solution.py:104
  143.7 2.2 convolution_multiply_fusion.4
  147.5 2.3 while.13
  149.9 1.7 multiply_reduce_fusion
  152.0 41.4 %all-gather.16.cloned.1.call-done = bf16[2048,512]{1,0:T(8,128)(2,1)} async-done(((bf16[256,512]{1,0:T(8,128)(2,1)}), bf16[2048,512]{1,0:T(8,128)(2,1)}) %all-gather.16.cloned.1.call-update) | async-done | bytes 2097168 | tf_op jit(solution)/shard_map/all_gather | solution.py:105
  193.4 50.8 %all-gather.18.cloned.1.call-done = bf16[512,2048]{1,0:T(8,128)(2,1)} async-done(((bf16[512,256]{1,0:T(8,128)(2,1)}), bf16[512,2048]{1,0:T(8,128)(2,1)}) %all-gather.18.cloned.1.call-update) | async-done | bytes 2097168 | tf_op jit(solution)/shard_map/all_gather | solution.py:106
  244.4 4.3 fusion.6
  248.8 3.8 convert_element_type.80
  252.7 3.8 convert_element_type.82
  257.2 17.9 %all-gather.1 = f32[8,1,256]{2,1,0:T(1,128)S(1)} all-gather(f32[1,1,256]{2,1,0:T(1,128)S(1)} %bitcast.110), channel_id=1, replica_groups=mesh['rep'=2,'fs'=8,'tp'=2] {'fs'}, dimensions={0}, use_global_device_ids=true | all-gather | bytes 9216 | tf_op jit(solution)/shard_map/all_gather | solution.py:110
  276.3 2.4 all_gather.40
  278.9 207.0 %all-gather.20.cloned.1.call-done = bf16[2048,4096]{1,0:T(8,128)(2,1)} async-done(((bf16[256,4096]{1,0:T(8,128)(2,1)}), bf16[2048,4096]{1,0:T(8,128)(2,1)}) %all-gather.20.cloned.1.call-update) | async-done | bytes 16777232 | tf_op jit(solution)/shard_map/all_gather | solution.py:136
  485.9 227.6 %all-gather.22.cloned.1.call-done = bf16[4096,2048]{1,0:T(8,128)(2,1)} async-done(((bf16[4096,256]{1,0:T(8,128)(2,1)}), bf16[4096,2048]{1,0:T(8,128)(2,1)}) %all-gather.22.cloned.1.call-update) | async-done | bytes 16777232 | tf_op jit(solution)/shard_map/all_gather | solution.py:137
  713.4 15.1 %fusion.5 = bf16[2048,192]{0,1:T(8,128)(2,1)} fusion(bf16[4096,2048]{1,0:T(8,128)(2,1)} %all-gather.22.cloned.1.call-done, f32[2048]{0:T(1024)S(1)} %bitcast.108, bf16[2048,4096]{1,0:T(8,128)(2,1)} %all-gather.20.cloned.1.call-done, f32[4096]{0:T(1024)S(1)} %copy-done.6, bf16[192,2048]{1,0:T(8,128)(2,1)S(1)} %all_gather.40, f32[2048]{0:T(1024)S(1)} %copy-done.8, ...), kind=kOutput, calls=%fused_computation.10 | convolution fusion | flops 6447955968 | bytes 35160832 | tf_op jit(solution)/shard_map/dot_general | solution.py:75
  728.5 6.5 reduce-scatter.5.cloned.1.call-done
  735.0 1.9 fusion.15
  (84 shorter events, 12.4 us)
Async XLA Ops:
  6.5 5.4 copy-start.1
  6.5 6.3 copy-start.2
  6.5 46.1 %all-gather.10.cloned.1.call-start = ((), (), s32[]{:S(2)}) async-start(), calls=%async_computation.2 | async-start | bytes 1179648 | tf_op jit(solution)/shard_map/all_gather | solution.py:102
  8.3 85.5 %all-gather.12.cloned.1.call-start = ((), (), s32[]{:S(2)}) async-start(), calls=%async_computation.3 | async-start | bytes 1179648 | tf_op jit(solution)/shard_map/all_gather | solution.py:103
  10.0 3.8 copy-start
  10.0 133.7 %all-gather.14.cloned.1.call-start = ((), (), s32[]{:S(2)}) async-start(), calls=%async_computation.4 | async-start | bytes 2359296 | tf_op jit(solution)/shard_map/all_gather | solution.py:104
  11.9 181.5 %all-gather.16.cloned.1.call-start = ((), (), s32[]{:S(2)}) async-start(), calls=%async_computation.5 | async-start | bytes 2359296 | tf_op jit(solution)/shard_map/all_gather | solution.py:105
  12.7 4.1 copy-start.3
  12.7 4.3 copy-start.4
  12.8 39.9 %copy-start.7 = (f32[2048]{0:T(1024)S(1)}, f32[2048]{0:T(1024)}, u32[]{:S(2)}) copy-start(f32[2048]{0:T(1024)} %param.23) | copy-start | bytes 24580
  12.8 39.9 %copy-start.11 = (f32[256]{0:T(256)S(1)}, f32[256]{0:T(256)}, u32[]{:S(2)}) copy-start(f32[256]{0:T(256)} %param.26) | copy-start | bytes 3076
  12.8 231.4 %all-gather.18.cloned.1.call-start = ((), (), s32[]{:S(2)}) async-start(), calls=%async_computation.6 | async-start | bytes 2359296 | tf_op jit(solution)/shard_map/all_gather | solution.py:106
  13.6 261.5 %reduce-scatter.3.cloned.1.call-start = ((), (), s32[]{:S(2)}) async-start(), calls=%async_computation.7 | async-start | bytes 1179648 | tf_op jit(solution)/shard_map/reduce_scatter | solution.py:127
  16.9 76.9 %copy-start.12 = (f32[256]{0:T(256)S(1)}, f32[256]{0:T(256)}, u32[]{:S(2)}) copy-start(f32[256]{0:T(256)} %param.28) | copy-start | bytes 3076
  95.7 48.1 %copy-start.9 = (f32[512]{0:T(512)S(1)}, f32[512]{0:T(512)}, u32[]{:S(2)}) copy-start(f32[512]{0:T(512)} %param.30) | copy-start | bytes 6148
  149.8 94.6 %copy-start.10 = (f32[512]{0:T(512)S(1)}, f32[512]{0:T(512)}, u32[]{:S(2)}) copy-start(f32[512]{0:T(512)} %param.32) | copy-start | bytes 6148
  248.8 237.1 %all-gather.20.cloned.1.call-start = ((), (), s32[]{:S(2)}) async-start(), calls=%async_computation.8 | async-start | bytes 18874368 | tf_op jit(solution)/shard_map/all_gather | solution.py:136
  252.6 460.8 %all-gather.22.cloned.1.call-start = ((), (), s32[]{:S(2)}) async-start(), calls=%async_computation.9 | async-start | bytes 18874368 | tf_op jit(solution)/shard_map/all_gather | solution.py:137
  256.5 0.7 copy-start.5
  256.5 478.5 %reduce-scatter.5.cloned.1.call-start = ((), (), s32[]{:S(2)}) async-start(), calls=%async_computation.10 | async-start | bytes 1179648 | tf_op jit(solution)/shard_map/reduce_scatter | solution.py:141
  275.1 438.3 %copy-start.6 = (f32[4096]{0:T(1024)S(1)}, f32[4096]{0:T(1024)}, u32[]{:S(2)}) copy-start(f32[4096]{0:T(1024)} %param.36) | copy-start | bytes 49156
  275.1 438.3 %copy-start.8 = (f32[2048]{0:T(1024)S(1)}, f32[2048]{0:T(1024)}, u32[]{:S(2)}) copy-start(f32[2048]{0:T(1024)} %param.24) | copy-start | bytes 24580
Sparse Core Ops, SparseCore 0:
  9.5 43.1 all-gather.9
  54.7 38.9 all-gather.11
  95.9 47.7 all-gather.13
  145.7 47.6 all-gather.15
  195.2 48.8 all-gather.17
  248.9 6.3 reduce-scatter.2
  257.4 228.4 all-gather.19
  487.9 225.4 all-gather.21
  728.6 6.3 reduce-scatter.4
where the time goes:
time: 744 us; the launch traced here: 743 us
  waiting for transfers between devices  633 us (85%)
  blocking collectives  45 us (6%)
  matrix products  28.8 us (4%)
  other arithmetic  20.7 us (3%)
  between operations  13.5 us (2%)
    all_gather x1, waiting for transfers between devices, on_device(): lax.all_gather(down_weight.astype(jnp.bfloat16), 'fs', axis=1, tiled=True)  228 us
    all_gather x1, waiting for transfers between devices, on_device(): lax.all_gather(up_weight.astype(jnp.bfloat16), 'fs', axis=0, tiled=True)  207 us
    all_gather x1, waiting for transfers between devices, on_device(): lax.all_gather(out_weight.astype(jnp.bfloat16), 'fs', axis=1, tiled=True)  50.8 us
    all_gather x1, waiting for transfers between devices, on_device(): lax.all_gather(value_weight.astype(jnp.bfloat16), 'fs', axis=0, tiled=True)  46.9 us
    all_gather x1, waiting for transfers between devices, on_device(): lax.all_gather(gate_weight.astype(jnp.bfloat16), 'fs', axis=0, tiled=True)  41.4 us
    all_gather x1, waiting for transfers between devices, on_device(): lax.all_gather(key_weight.astype(jnp.bfloat16), 'fs', axis=0, tiled=True)  39.3 us
    all_gather x1, blocking collectives, on_device(): lax.all_gather(out_scale, 'fs', axis=0, tiled=True)  22.2 us
    dot_general x2, matrix products, column_terms(): lax.dot_general(weight, hidden, (((0,), (1,)), ((), ())), preferred_eleme...  19.4 us
  transfers between devices with their start and end apart: 9, of which 8 were waited for; matrix products, arithmetic and copies ran while one was open for 4% of the time, Pallas kernels for 0%

commit v1 on v0

--- a/solution.py
+++ b/solution.py
@@ -134,7 +134,7 @@
     normed_two = gather_norm(first, mlp_gain)
     up_full, down_full = (
         lax.all_gather(up_weight.astype(jnp.bfloat16), "fs", axis=0, tiled=True),
-        lax.all_gather(down_weight.astype(jnp.bfloat16), "fs", axis=1, tiled=True),
+        jnp.concatenate(lax.all_gather(down_weight.astype(jnp.bfloat16), "fs"), axis=1),
     )
     raised = jnp.dot(normed_two, up_full, preferred_element_type=jnp.float32) * up_scale
     hidden = jnp.square(jax.nn.relu(raised)).astype(jnp.bfloat16)

time: 744 us -> 746 us (level)
  waiting for transfers between devices: 633 us -> 610 us
  local copies, waits for them, and re-layouts: 2.06 us -> 23.3 us
    reshape x0 -> x1, local copies, waits for them, and re-layouts: none -> 21.2 us  [on_device(): jnp.concatenate(lax.all_gather(down_weight.astype(jnp.bfloat16), 'fs'), a...]
    all_gather x1, waiting for transfers between devices: 228 us -> 207 us  [on_device(): lax.all_gather(down_weight.astype(jnp.bfloat16), 'fs')]
  transfers between devices with their start and end apart: 9 -> 9, of which waited for: 8 -> 8; matrix products, arithmetic and copies ran while one was open for 4% -> 7% of each run, Pallas kernels for 0% -> 0%
where the time goes in v1:
time: 746 us; the launch traced here: 745 us
  waiting for transfers between devices  610 us (82%)
  blocking collectives  45.3 us (6%)
  matrix products  31.6 us (4%)
  local copies, waits for them, and re-layouts  23.3 us (3%)
  other arithmetic  20.5 us (3%)
  between operations  13.5 us (2%)
    all_gather x1, waiting for transfers between devices, on_device(): lax.all_gather(down_weight.astype(jnp.bfloat16), 'fs')  207 us
    all_gather x1, waiting for transfers between devices, on_device(): lax.all_gather(up_weight.astype(jnp.bfloat16), 'fs', axis=0, tiled=True)  206 us
    all_gather x1, waiting for transfers between devices, on_device(): lax.all_gather(out_weight.astype(jnp.bfloat16), 'fs', axis=1, tiled=True)  50.8 us
    all_gather x1, waiting for transfers between devices, on_device(): lax.all_gather(value_weight.astype(jnp.bfloat16), 'fs', axis=0, tiled=True)  46.1 us
    all_gather x1, waiting for transfers between devices, on_device(): lax.all_gather(gate_weight.astype(jnp.bfloat16), 'fs', axis=0, tiled=True)  40.4 us
    all_gather x1, waiting for transfers between devices, on_device(): lax.all_gather(key_weight.astype(jnp.bfloat16), 'fs', axis=0, tiled=True)  39.3 us
    all_gather x1, blocking collectives, on_device(): lax.all_gather(out_scale, 'fs', axis=0, tiled=True)  22.2 us
    reshape x1, local copies, waits for them, and re-layouts, on_device(): jnp.concatenate(lax.all_gather(down_weight.astype(jnp.bfloat16), 'fs'), a...  21.2 us
  transfers between devices with their start and end apart: 9, of which 8 were waited for; matrix products, arithmetic and copies ran while one was open for 7% of the time, Pallas kernels for 0%

profile of v1, /device:TPU:0, one launch (start us, length us, event | category | flops | bytes accessed | tf_op | source)
XLA Modules:
  0.0 744.5 jit_solution(16678650009503489152)
XLA Ops:
  6.5 1.7 convert_element_type.68
  10.0 1.8 convert_element_type.70
  13.7 2.5 all_gather.36
  16.9 22.2 %all-gather.1 = f32[8,1,256]{2,1,0:T(1,128)S(1)} all-gather(f32[1,1,256]{2,1,0:T(1,128)S(1)} %bitcast.115), channel_id=1, replica_groups=mesh['rep'=2,'fs'=8,'tp'=2] {'fs'}, dimensions={0}, use_global_device_ids=true | all-gather | bytes 9216 | tf_op jit(solution)/shard_map/all_gather | solution.py:109
  39.2 13.4 %all-gather.11.cloned.1.call-done = bf16[2048,256]{1,0:T(8,128)(2,1)} async-done(((bf16[256,256]{1,0:T(8,128)(2,1)}), bf16[2048,256]{1,0:T(8,128)(2,1)}) %all-gather.11.cloned.1.call-update) | async-done | bytes 1048592 | tf_op jit(solution)/shard_map/all_gather | solution.py:102
  54.4 39.3 %all-gather.13.cloned.1.call-done = bf16[2048,256]{1,0:T(8,128)(2,1)} async-done(((bf16[256,256]{1,0:T(8,128)(2,1)}), bf16[2048,256]{1,0:T(8,128)(2,1)}) %all-gather.13.cloned.1.call-update) | async-done | bytes 1048592 | tf_op jit(solution)/shard_map/all_gather | solution.py:103
  93.7 1.6 convolution_multiply_fusion.6
  97.6 46.1 %all-gather.15.cloned.1.call-done = bf16[2048,512]{1,0:T(8,128)(2,1)} async-done(((bf16[256,512]{1,0:T(8,128)(2,1)}), bf16[2048,512]{1,0:T(8,128)(2,1)}) %all-gather.15.cloned.1.call-update) | async-done | bytes 2097168 | tf_op jit(solution)/shard_map/all_gather | solution.py:104
  143.7 2.2 convolution_multiply_fusion.4
  148.5 2.3 while.13
  150.8 1.7 multiply_reduce_fusion
  152.9 40.4 %all-gather.17.cloned.1.call-done = bf16[2048,512]{1,0:T(8,128)(2,1)} async-done(((bf16[256,512]{1,0:T(8,128)(2,1)}), bf16[2048,512]{1,0:T(8,128)(2,1)}) %all-gather.17.cloned.1.call-update) | async-done | bytes 2097168 | tf_op jit(solution)/shard_map/all_gather | solution.py:105
  193.3 50.8 %all-gather.19.cloned.1.call-done = bf16[512,2048]{1,0:T(8,128)(2,1)} async-done(((bf16[512,256]{1,0:T(8,128)(2,1)}), bf16[512,2048]{1,0:T(8,128)(2,1)}) %all-gather.19.cloned.1.call-update) | async-done | bytes 2097168 | tf_op jit(solution)/shard_map/all_gather | solution.py:106
  244.4 4.3 fusion.6
  248.8 3.7 convert_element_type.82
  252.6 3.9 convert_element_type.80
  257.1 18.0 %all-gather.2 = f32[8,1,256]{2,1,0:T(1,128)S(1)} all-gather(f32[1,1,256]{2,1,0:T(1,128)S(1)} %bitcast.116), channel_id=1, replica_groups=mesh['rep'=2,'fs'=8,'tp'=2] {'fs'}, dimensions={0}, use_global_device_ids=true | all-gather | bytes 9216 | tf_op jit(solution)/shard_map/all_gather | solution.py:110
  276.2 2.5 all_gather.43
  279.0 206.8 %all-gather.23.cloned.1.call-done = bf16[32768,256]{1,0:T(8,128)(2,1)} async-done(((bf16[4096,256]{1,0:T(8,128)(2,1)}), bf16[32768,256]{1,0:T(8,128)(2,1)}) %all-gather.23.cloned.1.call-update) | async-done | bytes 16777232 | tf_op jit(solution)/shard_map/all_gather | solution.py:137
  485.8 21.2 %copy.68 = bf16[4096,8,256]{0,2,1:T(8,128)(2,1)} copy(bf16[4096,8,256]{2,0,1:T(8,128)(2,1)} %bitcast.101) | data formatting | bytes 33554432 | tf_op jit(solution)/shard_map/reshape | solution.py:137
  507.0 206.4 %all-gather.21.cloned.1.call-done = bf16[2048,4096]{1,0:T(8,128)(2,1)} async-done(((bf16[256,4096]{1,0:T(8,128)(2,1)}), bf16[2048,4096]{1,0:T(8,128)(2,1)}) %all-gather.21.cloned.1.call-update) | async-done | bytes 16777232 | tf_op jit(solution)/shard_map/all_gather | solution.py:136
  713.4 16.2 %fusion.5 = bf16[2048,192]{0,1:T(8,128)(2,1)} fusion(bf16[4096,2048]{0,1:T(8,128)(2,1)} %bitcast.102, f32[2048]{0:T(1024)S(1)} %bitcast.114, bf16[2048,4096]{1,0:T(8,128)(2,1)} %all-gather.21.cloned.1.call-done, f32[4096]{0:T(1024)S(1)} %copy-done.6, bf16[192,2048]{1,0:T(8,128)(2,1)S(1)} %all_gather.43, f32[2048]{0:T(1024)S(1)} %copy-done.8, ...), kind=kOutput, calls=%fused_computation.10 | convolution fusion | flops 6447955968 | bytes 35160832 | tf_op jit(solution)/shard_map/dot_general | solution.py:75
  729.6 6.5 reduce-scatter.5.cloned.1.call-done
  736.1 1.9 fusion.15
  (85 shorter events, 15.7 us)
Async XLA Ops:
  6.5 5.4 copy-start.1
  6.5 6.3 copy-start.2
  6.5 46.1 %all-gather.11.cloned.1.call-start = ((), (), s32[]{:S(2)}) async-start(), calls=%async_computation.2 | async-start | bytes 1179648 | tf_op jit(solution)/shard_map/all_gather | solution.py:102
  8.3 85.5 %all-gather.13.cloned.1.call-start = ((), (), s32[]{:S(2)}) async-start(), calls=%async_computation.3 | async-start | bytes 1179648 | tf_op jit(solution)/shard_map/all_gather | solution.py:103
  10.0 3.7 copy-start
  10.0 133.7 %all-gather.15.cloned.1.call-start = ((), (), s32[]{:S(2)}) async-start(), calls=%async_computation.4 | async-start | bytes 2359296 | tf_op jit(solution)/shard_map/all_gather | solution.py:104
  11.9 181.5 %all-gather.17.cloned.1.call-start = ((), (), s32[]{:S(2)}) async-start(), calls=%async_computation.5 | async-start | bytes 2359296 | tf_op jit(solution)/shard_map/all_gather | solution.py:105
  12.7 4.0 copy-start.3
  12.7 4.2 copy-start.4
  12.7 39.9 %copy-start.7 = (f32[2048]{0:T(1024)S(1)}, f32[2048]{0:T(1024)}, u32[]{:S(2)}) copy-start(f32[2048]{0:T(1024)} %param.23) | copy-start | bytes 24580
  12.7 39.9 %copy-start.11 = (f32[256]{0:T(256)S(1)}, f32[256]{0:T(256)}, u32[]{:S(2)}) copy-start(f32[256]{0:T(256)} %param.26) | copy-start | bytes 3076
  12.7 231.4 %all-gather.19.cloned.1.call-start = ((), (), s32[]{:S(2)}) async-start(), calls=%async_computation.6 | async-start | bytes 2359296 | tf_op jit(solution)/shard_map/all_gather | solution.py:106
  13.6 261.6 %reduce-scatter.3.cloned.1.call-start = ((), (), s32[]{:S(2)}) async-start(), calls=%async_computation.7 | async-start | bytes 1179648 | tf_op jit(solution)/shard_map/reduce_scatter | solution.py:127
  16.7 77.0 %copy-start.12 = (f32[256]{0:T(256)S(1)}, f32[256]{0:T(256)}, u32[]{:S(2)}) copy-start(f32[256]{0:T(256)} %param.28) | copy-start | bytes 3076
  95.7 48.1 %copy-start.9 = (f32[512]{0:T(512)S(1)}, f32[512]{0:T(512)}, u32[]{:S(2)}) copy-start(f32[512]{0:T(512)} %param.30) | copy-start | bytes 6148
  150.8 93.6 %copy-start.10 = (f32[512]{0:T(512)S(1)}, f32[512]{0:T(512)}, u32[]{:S(2)}) copy-start(f32[512]{0:T(512)} %param.32) | copy-start | bytes 6148
  248.7 237.1 %all-gather.23.cloned.1.call-start = ((), (), s32[]{:S(2)}) async-start(), calls=%async_computation.10 | async-start | bytes 18874368 | tf_op jit(solution)/shard_map/all_gather | solution.py:137
  252.5 460.9 %all-gather.21.cloned.1.call-start = ((), (), s32[]{:S(2)}) async-start(), calls=%async_computation.8 | async-start | bytes 18874368 | tf_op jit(solution)/shard_map/all_gather | solution.py:136
  256.4 0.7 copy-start.5
  256.4 479.7 %reduce-scatter.5.cloned.1.call-start = ((), (), s32[]{:S(2)}) async-start(), calls=%async_computation.9 | async-start | bytes 1179648 | tf_op jit(solution)/shard_map/reduce_scatter | solution.py:141
  485.8 227.6 %copy-start.6 = (f32[4096]{0:T(1024)S(1)}, f32[4096]{0:T(1024)}, u32[]{:S(2)}) copy-start(f32[4096]{0:T(1024)} %param.36) | copy-start | bytes 49156
  485.8 227.6 %copy-start.8 = (f32[2048]{0:T(1024)S(1)}, f32[2048]{0:T(1024)}, u32[]{:S(2)}) copy-start(f32[2048]{0:T(1024)} %param.24) | copy-start | bytes 24580
Sparse Core Ops, SparseCore 0:
  9.5 43.0 all-gather.10
  54.7 38.9 all-gather.12
  95.9 47.7 all-gather.14
  145.7 47.6 all-gather.16
  195.2 48.8 all-gather.18
  248.9 6.3 reduce-scatter.2
  257.4 228.4 all-gather.22
  487.9 225.4 all-gather.20
  729.7 6.3 reduce-scatter.4
